TPU v7x, 32 devices: a whole 2x2x4 slice. The times are simulated.
32 devices in a mesh: grp: 2 (over x), ep: 8 (over z, y), tp: 2 (over core).
Axes of the slice: x: 2, y: 2, z: 4, core: 2. Of those that a mesh axis runs over, the one named last changes fastest.
Arguments:
- tokens: bfloat16 [1024, 1024], P(('grp', 'ep')), parts along dimension 0, may hold values from -6 to 6
- routes: int32 [1024, 4], P(('grp', 'ep')), parts along dimension 0, may hold values from 0 to 7, all different within a row; in each aligned block of 64 rows (0 to 63, 64 to 127, ...) at most 64 rows name the same one
- gates: float32 [1024, 4], P(('grp', 'ep')), parts along dimension 0, may hold values from 0.05 to 1
- norm_gain: float32 [1024], replicated, may hold values from 0.1 to 1.9
- w_gate: bfloat16 [8, 1024, 1792], P('ep', None, 'tp'), may hold values from -0.1875 to 0.1875
- w_up: bfloat16 [8, 1024, 1792], P('ep', None, 'tp'), may hold values from -0.1875 to 0.1875
- w_down: bfloat16 [8, 1792, 1024], P('ep', 'tp'), may hold values from -0.125 to 0.125
Outputs:
- mixed: bfloat16 [1024, 1024], P(('grp', 'ep')), parts along dimension 0
There are 2 independent parts, one for each index of `grp`. A program takes and returns all parts, laid end to end along the dimension named above; an argument that names none is the same for every part. Nothing has to cross between parts.
Inputs may be any that keep to these rules, and one draw needn't show every extreme that they name: `routes`: within the rows of one index of ep no expert is named more than 64 times; some expert is named exactly 64 times there in some or all of them.
All inputs are finite; a program needn't handle non-finite values.
Results may differ from a plain program's by a relative error of at most 0.0078.
Values may be sent and summed in bfloat16 or wider, within the bound.
A program may use at most 64 MiB of HBM per device.

v0:
```python
import jax
import jax.numpy as jnp
from jax import lax
from jax.sharding import PartitionSpec as P

EPS = 1e-06


def per_device(tokens, routes, gates, norm_gain, w_gate, w_up, w_down):
    tok_rows, width = tokens.shape
    top = routes.shape[1]
    ep_count = lax.axis_size("ep")
    tp_count = lax.axis_size("tp")
    capacity = max(2, min(tok_rows, 3 * tok_rows * top // ep_count))
    share = width // tp_count
    lane = lax.axis_index("tp")
    xf = tokens.astype(jnp.float32)
    normed = (xf * lax.rsqrt(jnp.mean(xf * xf, axis=-1, keepdims=True) + EPS) * norm_gain).astype(
        jnp.bfloat16
    )
    flat = routes.reshape(-1)
    onehot = (flat[:, None] == jnp.arange(ep_count, dtype=jnp.int32)[None, :]).astype(jnp.int32)
    earlier = jnp.cumsum(onehot, axis=0) - onehot
    rank = jnp.sum(earlier * onehot, axis=1)
    slot = flat * capacity + rank
    placing = (jnp.arange(ep_count * capacity, dtype=jnp.int32)[:, None] == slot[None, :]).astype(
        jnp.bfloat16
    )
    repeated = jnp.repeat(normed, top, axis=0)
    outgoing = jnp.dot(placing, repeated, preferred_element_type=jnp.float32).astype(jnp.bfloat16)
    outgoing = outgoing.reshape(ep_count, capacity, width)
    mine = lax.dynamic_slice_in_dim(outgoing, lane * share, share, 2)
    full = lax.all_gather(
        lax.all_to_all(mine, "ep", split_axis=0, concat_axis=0, tiled=True),
        "tp",
        axis=2,
        tiled=True,
    )
    sources = full.shape[0]
    items = full.shape[1]
    rows = full.reshape(sources * items, width)
    gate_act = jnp.dot(rows, w_gate[0], preferred_element_type=jnp.float32)
    up_act = jnp.dot(rows, w_up[0], preferred_element_type=jnp.float32)
    hidden = (jax.nn.silu(gate_act) * up_act).astype(jnp.bfloat16)
    partial_value = jnp.dot(hidden, w_down[0], preferred_element_type=jnp.float32).astype(
        jnp.bfloat16
    )
    summed = lax.psum_scatter(
        lax.optimization_barrier(partial_value)
        .astype(jnp.float32)
        .reshape(sources, items, width)
        .astype(jnp.bfloat16),
        "tp",
        scatter_dimension=2,
        tiled=True,
    )
    returned = lax.all_to_all(summed, "ep", split_axis=0, concat_axis=0, tiled=True)
    back = returned.reshape(ep_count * capacity, returned.shape[2])
    picked = jnp.take(back, slot, axis=0).reshape(tok_rows, top, back.shape[1])
    mixed = jnp.sum(gates[:, :, None] * picked.astype(jnp.float32), axis=1).astype(jnp.bfloat16)
    mixed = lax.all_gather(mixed, "tp", axis=1, tiled=True)
    return mixed


def solution(mesh):
    return jax.shard_map(
        per_device,
        mesh=mesh,
        in_specs=(
            P(("grp", "ep"), None),
            P(("grp", "ep"), None),
            P(("grp", "ep"), None),
            P(),
            P("ep", None, "tp"),
            P("ep", None, "tp"),
            P("ep", "tp", None),
        ),
        out_specs=P(("grp", "ep"), None),
        check_vma=False,
    )
```

profile of v0, /device:TPU:0, one launch (start us, length us, event | category | flops | bytes accessed | tf_op | source)
XLA Modules:
  0.0 92.8 jit_solution(17781713339959513913)
XLA Ops:
  6.5 0.0 copy-start
  6.5 0.0 all-gather.2.cloned.1.call-start
  6.5 0.9 copy.15
  7.4 0.1 eq.39
  7.5 0.1 reshape.94
  7.7 0.6 reduce-window.6
  8.3 0.2 slice_reduce_fusion
  8.5 0.1 fusion.19
  8.6 1.0 %fusion.14 = f32[64]{0:T(128)S(1)} fusion(bf16[64,1024]{1,0:T(8,128)(2,1)} %param.7), kind=kLoop, calls=%fused_computation.15 | loop fusion | flops 196544 | bytes 131328 | tf_op jit(solution)/shard_map/reduce_sum | solution.py:18
  9.7 1.0 %fusion.16 = bf16[64,1024]{1,0:T(8,128)(2,1)S(1)} fusion(bf16[64,1024]{1,0:T(8,128)(2,1)} %param.7, f32[1024]{0:T(1024)} %param.10, f32[64]{0:T(128)S(1)} %add_rsqrt_fusion), kind=kLoop, calls=%fused_computation.17 | loop fusion | flops 262144 | bytes 266496 | tf_op jit(solution)/shard_map/convert_element_type | solution.py:18
  10.7 0.2 broadcast_in_dim.20
  10.9 0.1 reshape.96
  11.0 0.4 convolution_convert_fusion
  11.5 21.7 %all_to_all.10 = bf16[8,64,512]{2,1,0:T(8,128)(2,1)} all-to-all(bf16[8,64,512]{2,1,0:T(8,128)(2,1)S(1)} %constant_dynamic-slice_fusion), channel_id=1, replica_groups=mesh['grp'=2,'ep'=8,'tp'=2] {'ep'}, dimensions={0} | all-to-all | bytes 1048576 | tf_op jit(solution)/shard_map/all_to_all | solution.py:34
  33.2 0.0 all-gather.2.cloned.1.call-update
  33.3 0.0 reduce-scatter.2.cloned.1.call-start
  33.3 8.1 %all-gather.2.cloned.1.call-done = bf16[8,64,1024]{2,1,0:T(8,128)(2,1)} async-done(((bf16[8,64,512]{2,1,0:T(8,128)(2,1)}), bf16[8,64,1024]{2,1,0:T(8,128)(2,1)}) %all-gather.2.cloned.1.call-update) | async-done | bytes 1048592 | tf_op jit(solution)/shard_map/all_gather | solution.py:33
  41.4 0.0 copy-start.3
  41.4 4.4 %fusion.4 = f32[512,896]{1,0:T(8,128)} fusion(bf16[512,1024]{1,0:T(8,128)(2,1)} %bitcast.37, bf16[1,1024,896]{2,1,0:T(8,128)(2,1)} %param.11), kind=kOutput, calls=%fused_computation.5 | convolution fusion | flops 939524096 | bytes 4718592 | tf_op jit(solution)/shard_map/dot_general | solution.py:42
  45.9 0.0 copy-done
  45.9 0.0 copy-done.3
  45.9 5.4 %fusion.8 = bf16[512,1024]{1,0:T(8,128)(2,1)} fusion(bf16[1,896,1024]{2,1,0:T(8,128)(2,1)S(1)} %copy-done, f32[512,896]{1,0:T(8,128)} %fusion.4, bf16[512,1024]{1,0:T(8,128)(2,1)S(1)} %bitcast.38, bf16[1,1024,896]{2,1,0:T(8,128)(2,1)} %param.12), kind=kOutput, calls=%fused_computation.8 | convolution fusion | flops 1882324992 | bytes 7602176 | tf_op jit(solution)/shard_map/dot_general | solution.py:45
  51.3 0.0 copy-start.1
  51.3 0.0 copy-start.2
  51.3 0.0 reduce-scatter.2.cloned.1.call-update
  51.3 9.7 %reduce-scatter.2.cloned.1.call-done = bf16[8,64,512]{2,1,0:T(8,128)(2,1)} async-done(((bf16[8,64,1024]{2,1,0:T(8,128)(2,1)}), bf16[8,64,512]{2,1,0:T(8,128)(2,1)}) %reduce-scatter.2.cloned.1.call-update) | async-done | bytes 524304 | tf_op jit(solution)/shard_map/reduce_scatter | solution.py:48
  61.0 5.8 %all-to-all-start.1 = ((bf16[8,64,512]{2,1,0:T(8,128)(2,1)}), bf16[8,64,512]{2,1,0:T(8,128)(2,1)S(1)}, u32[]{:S(2)}, u32[]{:S(2)}) async-start(bf16[8,64,512]{2,1,0:T(8,128)(2,1)} %reduce-scatter.2.cloned.1.call-done), calls=%async_computation.2 | async-start | bytes 1048576 | tf_op jit(solution)/shard_map/all_to_all | solution.py:57
  66.8 0.1 reduce_sum.32
  66.9 0.0 copy-done.1
  66.9 0.1 copy.19
  67.0 0.1 mul.81
  67.1 0.1 copy.17
  67.2 0.1 copy.18
  67.3 0.0 copy-done.2
  67.3 0.1 copy.14
  67.4 14.3 %all-to-all-done.1 = bf16[8,64,512]{2,1,0:T(8,128)(2,1)S(1)} async-done(((bf16[8,64,512]{2,1,0:T(8,128)(2,1)}), bf16[8,64,512]{2,1,0:T(8,128)(2,1)S(1)}, u32[]{:S(2)}, u32[]{:S(2)}) %all-to-all-start.1) | async-done | bytes 524320 | tf_op jit(solution)/shard_map/all_to_all | solution.py:57
  81.7 1.2 %gather_fusion = bf16[256,512]{1,0:T(8,128)(2,1)S(1)} fusion(bf16[512,512]{1,0:T(8,128)(2,1)S(1)} %bitcast.32, s32[1024]{0:T(1024)S(1)} %pad_clamp_fusion), kind=kCustom, calls=%fused_computation | custom fusion | bytes 525312 | tf_op jit(solution)/shard_map/jit(_take)/gather | solution.py:59
  82.9 0.1 gather.7
  83.0 0.5 multiply_reduce_fusion
  83.4 1.9 %all_gather.7 = bf16[64,1024]{1,0:T(8,128)(2,1)S(1)} all-gather(bf16[64,512]{1,0:T(8,128)(2,1)S(1)} %multiply_reduce_fusion), channel_id=1, replica_groups=mesh['grp'=2,'ep'=8,'tp'=2] {'tp'}, dimensions={1}, use_global_device_ids=true | all-gather | bytes 196608 | tf_op jit(solution)/shard_map/all_gather | solution.py:61
  85.3 0.7 copy.21
  (10 shorter events, 0.1 us)
Async XLA Ops:
  6.5 39.3 %copy-start = (bf16[1,896,1024]{2,1,0:T(8,128)(2,1)S(1)}, bf16[1,896,1024]{2,1,0:T(8,128)(2,1)}, u32[]{:S(2)}) copy-start(bf16[1,896,1024]{2,1,0:T(8,128)(2,1)} %param.13) | copy-start | bytes 5505028
  6.5 34.9 %all-gather.2.cloned.1.call-start = ((), (), s32[]{:S(2)}) async-start(), calls=%async_computation.3 | async-start | bytes 1572864 | tf_op jit(solution)/shard_map/all_gather | solution.py:33
  33.3 27.8 %reduce-scatter.2.cloned.1.call-start = ((), (), s32[]{:S(2)}) async-start(), calls=%async_computation.4 | async-start | bytes 1572864 | tf_op jit(solution)/shard_map/reduce_scatter | solution.py:48
  41.4 4.4 %copy-start.3 = (bf16[8,64,1024]{2,1,0:T(8,128)(2,1)S(1)}, bf16[8,64,1024]{2,1,0:T(8,128)(2,1)}, u32[]{:S(2)}) copy-start(bf16[8,64,1024]{2,1,0:T(8,128)(2,1)} %all-gather.2.cloned.1.call-done) | copy-start | bytes 3145732
  51.3 15.6 %copy-start.1 = (s32[64,4]{0,1:T(4,128)S(1)}, s32[64,4]{0,1:T(4,128)}, u32[]{:S(2)}) copy-start(s32[64,4]{0,1:T(4,128)} %param.8) | copy-start | bytes 3076
  51.3 16.1 %copy-start.2 = (f32[64,4]{0,1:T(4,128)S(1)}, f32[64,4]{0,1:T(4,128)}, u32[]{:S(2)}) copy-start(f32[64,4]{0,1:T(4,128)} %param.9) | copy-start | bytes 3076
  61.0 20.7 %all-to-all-start.1 = ((bf16[8,64,512]{2,1,0:T(8,128)(2,1)}), bf16[8,64,512]{2,1,0:T(8,128)(2,1)S(1)}, u32[]{:S(2)}, u32[]{:S(2)}) async-start(bf16[8,64,512]{2,1,0:T(8,128)(2,1)} %reduce-scatter.2.cloned.1.call-done), calls=%async_computation.2 | async-start | bytes 1048576 | tf_op jit(solution)/shard_map/all_to_all | solution.py:57
Sparse Core Ops, SparseCore 0:
  33.4 8.0 all-gather.1
  51.4 9.5 reduce-scatter.1
where the time goes:
time: 93.1 us; the launch traced here: 92.8 us
  waiting for transfers between devices  32.2 us (35%)
  blocking collectives  23.6 us (25%)
  between operations  13.5 us (15%)
  matrix products  10.3 us (11%)
  starting transfers between devices  5.8 us (6%)
  local copies, waits for them, and re-layouts  4.12 us (4%)
  other arithmetic  3.27 us (4%)
    all_to_all x1, blocking collectives, per_device(): lax.all_to_all(mine, 'ep', split_axis=0, concat_axis=0, tiled=True)  21.7 us
    all_to_all x1, waiting for transfers between devices, per_device(): lax.all_to_all(summed, 'ep', split_axis=0, concat_axis=0, tiled=True)  14.3 us
    reduce_scatter x1, waiting for transfers between devices, per_device(): lax.psum_scatter(lax.optimization_barrier(partial_value).astype(jnp.float...  9.73 us
    all_gather x1, waiting for transfers between devices, per_device(): lax.all_gather(lax.all_to_all(mine, 'ep', split_axis=0, concat_axis=0, ti...  8.13 us
    all_to_all x1, starting transfers between devices, per_device(): lax.all_to_all(summed, 'ep', split_axis=0, concat_axis=0, tiled=True)  5.75 us
    dot_general x1, matrix products, per_device(): jnp.dot(hidden, w_down[0], preferred_element_type=jnp.float32)  5.41 us
    dot_general x1, matrix products, per_device(): gate_act = jnp.dot(rows, w_gate[0], preferred_element_type=jnp.float32)  4.41 us
    all_gather x1, blocking collectives, per_device(): mixed = lax.all_gather(mixed, 'tp', axis=1, tiled=True)  1.9 us
  transfers between devices with their start and end apart: 3, of which 3 were waited for; matrix products, arithmetic and copies ran while one was open for 1% of the time, Pallas kernels for 0%

commit v1 on v0

--- a/solution.py
+++ b/solution.py
@@ -1,12 +1,218 @@
+import functools
+
 import jax
 import jax.numpy as jnp
 from jax import lax
+from jax.experimental import pallas as pl
+from jax.experimental.pallas import tpu as pltpu
 from jax.sharding import PartitionSpec as P
 
 EPS = 1e-06
-
-
-def per_device(tokens, routes, gates, norm_gain, w_gate, w_up, w_down):
+MESH = pl.DeviceIdType.MESH
+
+
+def flipped(value, bits):
+    result, bit = value, 1
+    while bit <= bits:
+        if bits & bit:
+            result = result + bit - 2 * bit * ((value // bit) % 2)
+        bit *= 2
+    return result
+
+
+def dense_kernel(
+    lines, tok_ref, route_ref, gate_ref, gain_ref, wg_hbm, wu_hbm, wd_hbm, out_ref,
+    wg, wu, wd, xg, gg, po, rd, ys, ry, zs, rz, keep, fin, ro,
+    w_sem, zx_s, zx_r, zg_s, zg_r, yx_s, yx_r, yg_s, yg_r, dx_s, dx_r,
+    rd_s, rd_r, ry_s, ry_r, rz_s, rz_r, ro_s, ro_r,
+):
+    rows, width = tok_ref.shape
+    half = rows // 2
+    grp, me, lane = lax.axis_index("grp"), lax.axis_index("ep"), lax.axis_index("tp")
+    line, col = me // 2, me % 2
+    peer_z = [(grp, flipped(line, k) * 2 + col, lane) for k in range(lines)]
+    peer_y = (grp, line * 2 + 1 - col, lane)
+    peer_c = (grp, me, 1 - lane)
+    sent = []
+
+    weights = [
+        pltpu.make_async_copy(src.at[0], dst, w_sem.at[i])
+        for i, (src, dst) in enumerate(((wg_hbm, wg), (wu_hbm, wu), (wd_hbm, wd)))
+    ]
+    for copy in weights:
+        copy.start()
+    barrier = pltpu.get_barrier_semaphore()
+    others = peer_z[1:] + [peer_y, peer_c]
+    for other in others:
+        pl.semaphore_signal(barrier, inc=1, device_id=other, device_id_type=MESH)
+
+    def remote(src, dst, send_sem, recv_sem, device):
+        copy = pltpu.make_async_remote_copy(
+            src_ref=src, dst_ref=dst, send_sem=send_sem, recv_sem=recv_sem,
+            device_id=device, device_id_type=MESH,
+        )
+        copy.start()
+        sent.append(copy)
+
+    def landed(ref, sem):
+        pltpu.make_async_remote_copy(
+            src_ref=ref, dst_ref=ref, send_sem=sem, recv_sem=sem,
+            device_id=peer_c, device_id_type=MESH,
+        ).wait_recv()
+
+    gain = gain_ref[...]
+    for part, first in ((0, lane * half), (1, (1 - lane) * half)):
+        xf = tok_ref[pl.ds(pl.multiple_of(first, half), half), :].astype(jnp.float32)
+        scale = lax.rsqrt(jnp.mean(xf * xf, axis=-1, keepdims=True) + EPS)
+        xg[0, part, 0] = (xf * scale * gain).astype(jnp.bfloat16)
+    pieces = []
+    for first in (lane * half, (1 - lane) * half):
+        window = pl.ds(pl.multiple_of(first, half), half)
+        names, scales = route_ref[window, :], gate_ref[window, :]
+        expert = lax.broadcasted_iota(jnp.int32, (half, 2 * rows), 1)
+        piece = jnp.zeros((half, 2 * rows), jnp.float32)
+        for k in range(names.shape[1]):
+            piece = piece + jnp.where(names[:, k:k + 1] == expert, scales[:, k:k + 1], 0.0)
+        pieces.append(piece)
+    table = jnp.concatenate(pieces + pieces, axis=0)
+    gg[0, 0] = jnp.transpose(table)[: gg.shape[2]]
+
+    pl.semaphore_wait(barrier, len(others))
+
+    def over_y(k):
+        remote(xg.at[k, 0, 0], xg.at[k, 0, 1], yx_s.at[k], yx_r.at[k], peer_y)
+        remote(gg.at[k, 0], gg.at[k, 1], yg_s.at[k], yg_r.at[k], peer_y)
+
+    def over_c(k, j):
+        remote(xg.at[k, 0, j], xg.at[k, 1, j], dx_s.at[k, j], dx_r.at[k, j], peer_c)
+
+    over_y(0)
+    for k in range(1, lines):
+        remote(xg.at[0, 0, 0], xg.at[k, 0, 0], zx_s.at[k], zx_r.at[k], peer_z[k])
+        remote(gg.at[0, 0], gg.at[k, 0], zg_s.at[k], zg_r.at[k], peer_z[k])
+
+    def from_z(k):
+        landed(xg.at[k, 0, 0], zx_r.at[k])
+        landed(gg.at[k, 0], zg_r.at[k])
+        over_y(k)
+        over_c(k, 0)
+
+    def from_y(k):
+        landed(xg.at[k, 0, 1], yx_r.at[k])
+        landed(gg.at[k, 1], yg_r.at[k])
+        over_c(k, 1)
+
+    def compute(k):
+        if k:
+            landed(xg.at[k, 1, 0], dx_r.at[k, 0])
+        landed(xg.at[k, 1, 1], dx_r.at[k, 1])
+        if k == 0:
+            weights[0].wait()
+            weights[1].wait()
+        count = 2 * rows
+        x = xg[k].reshape(count, width)
+        spot = lax.broadcasted_iota(jnp.int32, gg.shape[2:], 1)
+        first, second = gg[k, 0], gg[k, 1]
+        mine = lax.broadcasted_iota(jnp.int32, gg.shape[2:], 0) == me
+        row_a = jnp.sum(jnp.where(mine, first, 0.0), axis=0, keepdims=True)
+        row_b = jnp.sum(jnp.where(mine, second, 0.0), axis=0, keepdims=True)
+        at = lax.broadcasted_iota(jnp.int32, (count, count), 0)
+        token = (at // rows) * half + at % half
+        hit = lax.broadcasted_iota(jnp.int32, (count, count), 1) == token
+        column = (at // half) % 2
+        gate = jnp.sum(
+            jnp.where(hit, jnp.where(column == 0, row_a, row_b), 0.0), axis=1, keepdims=True
+        )
+        g = jnp.dot(x, wg[...], preferred_element_type=jnp.float32)
+        u = jnp.dot(x, wu[...], preferred_element_type=jnp.float32)
+        hidden = (g / (1.0 + jnp.exp(-g)) * u * gate).astype(jnp.bfloat16)
+        if k == 0:
+            weights[2].wait()
+        y = jnp.dot(hidden, wd[...], preferred_element_type=jnp.float32)
+        po[k] = y.astype(jnp.bfloat16).reshape(2, 2, half, width)
+        remote(po.at[k, 1], rd.at[k], rd_s.at[k], rd_r.at[k], peer_c)
+
+    def back_y(k):
+        landed(rd.at[k], rd_r.at[k])
+        ys[k] = (po[k, 0, 1].astype(jnp.float32) + rd[k, 1].astype(jnp.float32)).astype(jnp.bfloat16)
+        remote(ys.at[k], ry.at[k], ry_s.at[k], ry_r.at[k], peer_y)
+
+    def back_z(k):
+        landed(ry.at[k], ry_r.at[k])
+        total = (
+            po[k, 0, 0].astype(jnp.float32)
+            + rd[k, 0].astype(jnp.float32)
+            + ry[k].astype(jnp.float32)
+        )
+        if k == 0:
+            keep[...] = total
+        else:
+            zs[k] = total.astype(jnp.bfloat16)
+            remote(zs.at[k], rz.at[k], rz_s.at[k], rz_r.at[k], peer_z[k])
+
+    def step(fn, k, low=0):
+        if low <= k < lines:
+            fn(k)
+
+    for tick in range(lines + 3):
+        step(from_z, tick + 1, 1)
+        step(from_y, tick)
+        step(compute, tick - 1)
+        step(back_y, tick - 2)
+        step(back_z, tick - 3)
+    total = keep[...]
+    for k in range(1, lines):
+        landed(rz.at[k], rz_r.at[k])
+        total = total + rz[k].astype(jnp.float32)
+    fin[...] = total.astype(jnp.bfloat16)
+    remote(fin, ro, ro_s, ro_r, peer_c)
+    out_ref[pl.ds(pl.multiple_of(lane * half, half), half), :] = fin[...]
+    landed(ro, ro_r)
+    out_ref[pl.ds(pl.multiple_of((1 - lane) * half, half), half), :] = ro[...]
+    for copy in sent:
+        copy.wait_send()
+
+
+def dense_device(lines, tokens, routes, gates, norm_gain, w_gate, w_up, w_down):
+    rows, width = tokens.shape
+    half = rows // 2
+    units = w_gate.shape[2]
+    experts = lines * 2
+    bf16, f32 = jnp.bfloat16, jnp.float32
+    dma = pltpu.SemaphoreType.DMA
+    vmem, anywhere = pl.BlockSpec(memory_space=pltpu.VMEM), pl.BlockSpec(memory_space=pl.ANY)
+    return pl.pallas_call(
+        functools.partial(dense_kernel, lines),
+        out_shape=jax.ShapeDtypeStruct((rows, width), bf16),
+        in_specs=[vmem] * 4 + [anywhere] * 3,
+        out_specs=vmem,
+        scratch_shapes=[
+            pltpu.VMEM((width, units), bf16),
+            pltpu.VMEM((width, units), bf16),
+            pltpu.VMEM((units, width), bf16),
+            pltpu.VMEM((lines, 2, 2, half, width), bf16),
+            pltpu.VMEM((lines, 2, experts, 2 * rows), f32),
+            pltpu.VMEM((lines, 2, 2, half, width), bf16),
+            pltpu.VMEM((lines, 2, half, width), bf16),
+            pltpu.VMEM((lines, half, width), bf16),
+            pltpu.VMEM((lines, half, width), bf16),
+            pltpu.VMEM((lines, half, width), bf16),
+            pltpu.VMEM((lines, half, width), bf16),
+            pltpu.VMEM((half, width), f32),
+            pltpu.VMEM((half, width), bf16),
+            pltpu.VMEM((half, width), bf16),
+            dma((3,)),
+            dma((lines,)), dma((lines,)), dma((lines,)), dma((lines,)),
+            dma((lines,)), dma((lines,)), dma((lines,)), dma((lines,)),
+            dma((lines, 2)), dma((lines, 2)),
+            dma((lines,)), dma((lines,)), dma((lines,)), dma((lines,)),
+            dma((lines,)), dma((lines,)), dma, dma,
+        ],
+        compiler_params=pltpu.CompilerParams(collective_id=0, has_side_effects=True),
+    )(tokens, routes, gates, norm_gain.reshape(1, width), w_gate, w_up, w_down)
+
+
+def packed_device(tokens, routes, gates, norm_gain, w_gate, w_up, w_down):
     tok_rows, width = tokens.shape
     top = routes.shape[1]
     ep_count = lax.axis_size("ep")
@@ -60,6 +266,17 @@
     mixed = jnp.sum(gates[:, :, None] * picked.astype(jnp.float32), axis=1).astype(jnp.bfloat16)
     mixed = lax.all_gather(mixed, "tp", axis=1, tiled=True)
     return mixed
+
+
+def per_device(tokens, routes, gates, norm_gain, w_gate, w_up, w_down):
+    rows, width = tokens.shape
+    ep_count, tp_count = lax.axis_size("ep"), lax.axis_size("tp")
+    lines = ep_count // 2
+    whole = 3 * rows * routes.shape[1] // ep_count >= rows
+    fits = lines >= 2 and lines & (lines - 1) == 0 and lines * 2 == ep_count and ep_count % 8 == 0
+    if whole and fits and tp_count == 2 and rows % 64 == 0 and width % 128 == 0:
+        return dense_device(lines, tokens, routes, gates, norm_gain, w_gate, w_up, w_down)
+    return packed_device(tokens, routes, gates, norm_gain, w_gate, w_up, w_down)
 
 
 def solution(mesh):

time: 93.1 us -> 37.2 us (0.40)
  Pallas kernels: 0 us -> 32.7 us
  waiting for transfers between devices: 32.2 us -> 0 us
  blocking collectives: 23.6 us -> 0 us
  between operations: 13.5 us -> 0.01 us
  matrix products: 10.3 us -> 0 us
  starting transfers between devices: 5.8 us -> 0 us
  other arithmetic: 3.27 us -> 0 us
    pallas_call x0 -> x1, Pallas kernels: none -> 32.7 us  [dense_device(): pl.pallas_call(functools.partial(dense_kernel, lines), out_shape=jax.Shap...]
    all_to_all x1 -> x0, blocking collectives: 21.7 us -> none  [per_device(): lax.all_to_all(mine, 'ep', split_axis=0, concat_axis=0, tiled=True)]
    all_to_all x1 -> x0, waiting for transfers between devices: 14.3 us -> none  [per_device(): lax.all_to_all(summed, 'ep', split_axis=0, concat_axis=0, tiled=True)]
    dot_general x3 -> x0, matrix products: 10.3 us -> none  [the longest x1 5.41 us: per_device(): jnp.dot(hidden, w_down[0], preferred_element_type=jnp.float32)]
    reduce_scatter x1 -> x0, waiting for transfers between devices: 9.73 us -> none  [per_device(): lax.psum_scatter(lax.optimization_barrier(partial_value).astype(jnp.float...]
    all_gather x1 -> x0, waiting for transfers between devices: 8.13 us -> none  [per_device(): lax.all_gather(lax.all_to_all(mine, 'ep', split_axis=0, concat_axis=0, ti...]
    all_to_all x1 -> x0, starting transfers between devices: 5.75 us -> none  [per_device(): lax.all_to_all(summed, 'ep', split_axis=0, concat_axis=0, tiled=True)]
    unnamed x11 -> x3, local copies, waits for them, and re-layouts: 1.67 us -> 4.32 us
  transfers between devices with their start and end apart: 3 -> 0, of which waited for: 3 -> 0; matrix products, arithmetic and copies ran while one was open for 1% -> 0% of each run, Pallas kernels for 0% -> 0%
where the time goes in v1:
time: 37.2 us; the launch traced here: 37 us
  Pallas kernels  32.7 us (88%)
  local copies, waits for them, and re-layouts  4.32 us (12%)
    pallas_call x1, Pallas kernels, dense_device(): pl.pallas_call(functools.partial(dense_kernel, lines), out_shape=jax.Shap...  32.7 us
    unnamed x3, local copies, waits for them, and re-layouts  4.32 us

profile of v1, /device:TPU:0, one launch (start us, length us, event | category | flops | bytes accessed | tf_op | source)
XLA Modules:
  0.0 37.0 jit_solution(2438897782726019648)
XLA Ops:
  0.0 1.4 %copy.8.route_ref = s32[64,4]{1,0:T(8,128)} copy(s32[64,4]{0,1:T(4,128)} %param.8) | data formatting | bytes 2048 | tf_op args[1]
  1.4 1.4 %copy.9.gate_ref = f32[64,4]{1,0:T(8,128)} copy(f32[64,4]{0,1:T(4,128)} %param.9) | data formatting | bytes 2048 | tf_op args[2]
  2.8 32.7 %shard_map.73 = bf16[64,1024]{1,0:T(8,128)(2,1)} custom-call(bf16[64,1024]{1,0:T(8,128)(2,1)} %tok_ref.1, s32[64,4]{1,0:T(8,128)} %copy.8.route_ref, f32[64,4]{1,0:T(8,128)} %copy.9.gate_ref, f32[1,1024]{1,0:T(1,128)} %bitcast.1, bf16[1,1024,896]{2,1,0:T(8,128)(2,1)} %wg_hbm.1, bf16[1,1024,896]{2,1,0:T(8,128)(2,1)} %wu_hbm.1, bf16[1,896,1024]{2,1,0:T(8,128)(2,1)} %wd_hbm.1), custom_call_target="tpu_custom_call" | custom-call | tf_op jit(solution)/shard_map/pallas_call | solution.py:184
  35.5 1.6 %copy.11 = bf16[64,1024]{1,0:T(8,128)(2,1)} copy(bf16[64,1024]{1,0:T(8,128)(2,1)} %shard_map.73) | data formatting | bytes 262144

commit v2 on v1

--- a/solution.py
+++ b/solution.py
@@ -65,17 +65,14 @@
         xf = tok_ref[pl.ds(pl.multiple_of(first, half), half), :].astype(jnp.float32)
         scale = lax.rsqrt(jnp.mean(xf * xf, axis=-1, keepdims=True) + EPS)
         xg[0, part, 0] = (xf * scale * gain).astype(jnp.bfloat16)
-    pieces = []
-    for first in (lane * half, (1 - lane) * half):
-        window = pl.ds(pl.multiple_of(first, half), half)
-        names, scales = route_ref[window, :], gate_ref[window, :]
-        expert = lax.broadcasted_iota(jnp.int32, (half, 2 * rows), 1)
-        piece = jnp.zeros((half, 2 * rows), jnp.float32)
-        for k in range(names.shape[1]):
-            piece = piece + jnp.where(names[:, k:k + 1] == expert, scales[:, k:k + 1], 0.0)
-        pieces.append(piece)
-    table = jnp.concatenate(pieces + pieces, axis=0)
-    gg[0, 0] = jnp.transpose(table)[: gg.shape[2]]
+    names, scales = route_ref[...], gate_ref[...]
+    expert = lax.broadcasted_iota(jnp.int32, (gg.shape[2], rows), 0)
+    table = jnp.zeros((gg.shape[2], rows), jnp.float32)
+    for k in range(names.shape[0]):
+        table = table + jnp.where(names[k:k + 1] == expert, scales[k:k + 1], 0.0)
+    upper = jnp.concatenate([table[:, half:], table[:, :half]], axis=1)
+    table = jnp.where(lane == 0, table, upper)
+    gg[0, 0] = jnp.concatenate([table, table], axis=1)
 
     pl.semaphore_wait(barrier, len(others))
 
@@ -183,7 +180,7 @@
     vmem, anywhere = pl.BlockSpec(memory_space=pltpu.VMEM), pl.BlockSpec(memory_space=pl.ANY)
     return pl.pallas_call(
         functools.partial(dense_kernel, lines),
-        out_shape=jax.ShapeDtypeStruct((rows, width), bf16),
+        out_shape=pltpu.VMEM((rows, width), bf16),
         in_specs=[vmem] * 4 + [anywhere] * 3,
         out_specs=vmem,
         scratch_shapes=[
@@ -209,7 +206,7 @@
             dma((lines,)), dma((lines,)), dma, dma,
         ],
         compiler_params=pltpu.CompilerParams(collective_id=0, has_side_effects=True),
-    )(tokens, routes, gates, norm_gain.reshape(1, width), w_gate, w_up, w_down)
+    )(tokens, routes.T, gates.T, norm_gain.reshape(1, width), w_gate, w_up, w_down)
 
 
 def packed_device(tokens, routes, gates, norm_gain, w_gate, w_up, w_down):

time: 37.2 us -> 32.9 us (0.88)
  local copies, waits for them, and re-layouts: 4.32 us -> 0.66 us
  Pallas kernels: 32.7 us -> 32.1 us
    unnamed x3 -> x1, local copies, waits for them, and re-layouts: 4.32 us -> 0.66 us
    pallas_call x1, Pallas kernels: 32.7 us -> 32.1 us  [dense_device(): pl.pallas_call(functools.partial(dense_kernel, lines), out_shape=pltpu.VM...]
where the time goes in v2:
time: 32.9 us; the launch traced here: 32.7 us
  Pallas kernels  32.1 us (98%)
  local copies, waits for them, and re-layouts  0.66 us (2%)
    pallas_call x1, Pallas kernels, dense_device(): pl.pallas_call(functools.partial(dense_kernel, lines), out_shape=pltpu.VM...  32.1 us

profile of v2, /device:TPU:0, one launch (start us, length us, event | category | flops | bytes accessed | tf_op | source)
XLA Modules:
  0.0 32.7 jit_solution(4224739910819920133)
XLA Ops:
  0.0 32.1 %shard_map.73 = bf16[64,1024]{1,0:T(8,128)(2,1)S(1)} custom-call(bf16[64,1024]{1,0:T(8,128)(2,1)} %tok_ref.1, s32[4,64]{1,0:T(4,128)} %bitcast.4, f32[4,64]{1,0:T(4,128)} %bitcast.5, f32[1,1024]{1,0:T(1,128)} %bitcast.3, bf16[1,1024,896]{2,1,0:T(8,128)(2,1)} %wg_hbm.1, bf16[1,1024,896]{2,1,0:T(8,128)(2,1)} %wu_hbm.1, bf16[1,896,1024]{2,1,0:T(8,128)(2,1)} %wd_hbm.1), custom_call_target="tpu_custom_call" | custom-call | tf_op jit(solution)/shard_map/pallas_call | solution.py:181
  32.1 0.7 %copy.9 = bf16[64,1024]{1,0:T(8,128)(2,1)} copy(bf16[64,1024]{1,0:T(8,128)(2,1)S(1)} %shard_map.73) | data formatting | bytes 262144

commit v3 on v2

--- a/solution.py
+++ b/solution.py
@@ -9,6 +9,7 @@
 
 EPS = 1e-06
 MESH = pl.DeviceIdType.MESH
+PIECES = 1
 
 
 def flipped(value, bits):
@@ -42,7 +43,7 @@
     for copy in weights:
         copy.start()
     barrier = pltpu.get_barrier_semaphore()
-    others = peer_z[1:] + [peer_y, peer_c]
+    others = [peer_z[k] for k in range(1, lines) if k & (k - 1) == 0] + [peer_y, peer_c]
     for other in others:
         pl.semaphore_signal(barrier, inc=1, device_id=other, device_id_type=MESH)
 
@@ -76,28 +77,40 @@
 
     pl.semaphore_wait(barrier, len(others))
 
-    def over_y(k):
-        remote(xg.at[k, 0, 0], xg.at[k, 0, 1], yx_s.at[k], yx_r.at[k], peer_y)
-        remote(gg.at[k, 0], gg.at[k, 1], yg_s.at[k], yg_r.at[k], peer_y)
-
-    def over_c(k, j):
-        remote(xg.at[k, 0, j], xg.at[k, 1, j], dx_s.at[k, j], dx_r.at[k, j], peer_c)
-
-    over_y(0)
-    for k in range(1, lines):
-        remote(xg.at[0, 0, 0], xg.at[k, 0, 0], zx_s.at[k], zx_r.at[k], peer_z[k])
-        remote(gg.at[0, 0], gg.at[k, 0], zg_s.at[k], zg_r.at[k], peer_z[k])
+    cuts = [pl.ds(p * (half // PIECES), half // PIECES) for p in range(PIECES)]
+
+    def onward(k, p, cut):
+        bit = 1
+        while bit < lines:
+            if bit > k:
+                to = k + bit
+                remote(
+                    xg.at[k, 0, 0, cut], xg.at[to, 0, 0, cut], zx_s.at[to, p], zx_r.at[to, p],
+                    peer_z[bit],
+                )
+                if p == 0:
+                    remote(gg.at[k, 0], gg.at[to, 0], zg_s.at[to], zg_r.at[to], peer_z[bit])
+            bit *= 2
+        remote(xg.at[k, 0, 0, cut], xg.at[k, 0, 1, cut], yx_s.at[k, p], yx_r.at[k, p], peer_y)
+        if p == 0:
+            remote(gg.at[k, 0], gg.at[k, 1], yg_s.at[k], yg_r.at[k], peer_y)
+
+    for p, cut in enumerate(cuts):
+        onward(0, p, cut)
 
     def from_z(k):
-        landed(xg.at[k, 0, 0], zx_r.at[k])
-        landed(gg.at[k, 0], zg_r.at[k])
-        over_y(k)
-        over_c(k, 0)
+        for p, cut in enumerate(cuts):
+            landed(xg.at[k, 0, 0, cut], zx_r.at[k, p])
+            if p == 0:
+                landed(gg.at[k, 0], zg_r.at[k])
+            onward(k, p, cut)
+        remote(xg.at[k, 0, 0], xg.at[k, 1, 0], dx_s.at[k, 0], dx_r.at[k, 0], peer_c)
 
     def from_y(k):
-        landed(xg.at[k, 0, 1], yx_r.at[k])
         landed(gg.at[k, 1], yg_r.at[k])
-        over_c(k, 1)
+        for p, cut in enumerate(cuts):
+            landed(xg.at[k, 0, 1, cut], yx_r.at[k, p])
+        remote(xg.at[k, 0, 1], xg.at[k, 1, 1], dx_s.at[k, 1], dx_r.at[k, 1], peer_c)
 
     def compute(k):
         if k:
@@ -131,35 +144,50 @@
 
     def back_y(k):
         landed(rd.at[k], rd_r.at[k])
-        ys[k] = (po[k, 0, 1].astype(jnp.float32) + rd[k, 1].astype(jnp.float32)).astype(jnp.bfloat16)
-        remote(ys.at[k], ry.at[k], ry_s.at[k], ry_r.at[k], peer_y)
+        for p, cut in enumerate(cuts):
+            total = po[k, 0, 1, cut].astype(jnp.float32) + rd[k, 1, cut].astype(jnp.float32)
+            ys[k, cut] = total.astype(jnp.bfloat16)
+            remote(ys.at[k, cut], ry.at[k, cut], ry_s.at[k, p], ry_r.at[k, p], peer_y)
 
     def back_z(k):
-        landed(ry.at[k], ry_r.at[k])
-        total = (
-            po[k, 0, 0].astype(jnp.float32)
-            + rd[k, 0].astype(jnp.float32)
-            + ry[k].astype(jnp.float32)
-        )
-        if k == 0:
-            keep[...] = total
-        else:
-            zs[k] = total.astype(jnp.bfloat16)
-            remote(zs.at[k], rz.at[k], rz_s.at[k], rz_r.at[k], peer_z[k])
+        for p, cut in enumerate(cuts):
+            landed(ry.at[k, cut], ry_r.at[k, p])
+            total = (
+                po[k, 0, 0, cut].astype(jnp.float32)
+                + rd[k, 0, cut].astype(jnp.float32)
+                + ry[k, cut].astype(jnp.float32)
+            )
+            if k == 0:
+                keep[cut, :] = total
+            else:
+                zs[k, cut] = total.astype(jnp.bfloat16)
+                remote(zs.at[k, cut], rz.at[k, cut], rz_s.at[k, p], rz_r.at[k, p], peer_z[k])
 
     def step(fn, k, low=0):
         if low <= k < lines:
             fn(k)
 
-    for tick in range(lines + 3):
-        step(from_z, tick + 1, 1)
-        step(from_y, tick)
-        step(compute, tick - 1)
-        step(back_y, tick - 2)
-        step(back_z, tick - 3)
+    from_z(1)
+    from_y(0)
+    step(from_z, 2)
+    for k in range(lines):
+        compute(k)
+        if k < lines - 1:
+            step(back_y, k - 1)
+        step(from_y, k + 1)
+        step(from_z, k + 3)
+        if k == lines - 2:
+            back_y(k)
+    for k in range(1, lines - 2):
+        back_z(k)
+    back_y(lines - 1)
+    for k in range(max(1, lines - 2), lines):
+        back_z(k)
+    back_z(0)
     total = keep[...]
     for k in range(1, lines):
-        landed(rz.at[k], rz_r.at[k])
+        for p, cut in enumerate(cuts):
+            landed(rz.at[k, cut], rz_r.at[k, p])
         total = total + rz[k].astype(jnp.float32)
     fin[...] = total.astype(jnp.bfloat16)
     remote(fin, ro, ro_s, ro_r, peer_c)
@@ -177,6 +205,7 @@
     experts = lines * 2
     bf16, f32 = jnp.bfloat16, jnp.float32
     dma = pltpu.SemaphoreType.DMA
+    cut = dma((lines, PIECES))
     vmem, anywhere = pl.BlockSpec(memory_space=pltpu.VMEM), pl.BlockSpec(memory_space=pl.ANY)
     return pl.pallas_call(
         functools.partial(dense_kernel, lines),
@@ -199,11 +228,11 @@
             pltpu.VMEM((half, width), bf16),
             pltpu.VMEM((half, width), bf16),
             dma((3,)),
-            dma((lines,)), dma((lines,)), dma((lines,)), dma((lines,)),
-            dma((lines,)), dma((lines,)), dma((lines,)), dma((lines,)),
+            cut, cut, dma((lines,)), dma((lines,)),
+            cut, cut, dma((lines,)), dma((lines,)),
             dma((lines, 2)), dma((lines, 2)),
-            dma((lines,)), dma((lines,)), dma((lines,)), dma((lines,)),
-            dma((lines,)), dma((lines,)), dma, dma,
+            dma((lines,)), dma((lines,)), cut, cut,
+            cut, cut, dma, dma,
         ],
         compiler_params=pltpu.CompilerParams(collective_id=0, has_side_effects=True),
     )(tokens, routes.T, gates.T, norm_gain.reshape(1, width), w_gate, w_up, w_down)
@@ -270,7 +299,7 @@
     ep_count, tp_count = lax.axis_size("ep"), lax.axis_size("tp")
     lines = ep_count // 2
     whole = 3 * rows * routes.shape[1] // ep_count >= rows
-    fits = lines >= 2 and lines & (lines - 1) == 0 and lines * 2 == ep_count and ep_count % 8 == 0
+    fits = lines >= 4 and lines & (lines - 1) == 0 and lines * 2 == ep_count and ep_count % 8 == 0
     if whole and fits and tp_count == 2 and rows % 64 == 0 and width % 128 == 0:
         return dense_device(lines, tokens, routes, gates, norm_gain, w_gate, w_up, w_down)
     return packed_device(tokens, routes, gates, norm_gain, w_gate, w_up, w_down)

time: 32.9 us -> 31.1 us (0.945)
  Pallas kernels: 32.1 us -> 30.3 us
    pallas_call x1, Pallas kernels: 32.1 us -> 30.3 us  [dense_device(): pl.pallas_call(functools.partial(dense_kernel, lines), out_shape=pltpu.VM...]
where the time goes in v3:
time: 31.1 us; the launch traced here: 31 us
  Pallas kernels  30.3 us (97%)
  local copies, waits for them, and re-layouts  0.66 us (2%)
    pallas_call x1, Pallas kernels, dense_device(): pl.pallas_call(functools.partial(dense_kernel, lines), out_shape=pltpu.VM...  30.3 us
    unnamed x1, local copies, waits for them, and re-layouts  0.66 us

profile of v3, /device:TPU:0, one launch (start us, length us, event | category | flops | bytes accessed | tf_op | source)
XLA Modules:
  0.0 31.0 jit_solution(10800861910546434783)
XLA Ops:
  0.0 30.3 %shard_map.73 = bf16[64,1024]{1,0:T(8,128)(2,1)S(1)} custom-call(bf16[64,1024]{1,0:T(8,128)(2,1)} %tok_ref.1, s32[4,64]{1,0:T(4,128)} %bitcast.4, f32[4,64]{1,0:T(4,128)} %bitcast.5, f32[1,1024]{1,0:T(1,128)} %bitcast.3, bf16[1,1024,896]{2,1,0:T(8,128)(2,1)} %wg_hbm.1, bf16[1,1024,896]{2,1,0:T(8,128)(2,1)} %wu_hbm.1, bf16[1,896,1024]{2,1,0:T(8,128)(2,1)} %wd_hbm.1), custom_call_target="tpu_custom_call" | custom-call | tf_op jit(solution)/shard_map/pallas_call | solution.py:210
  30.3 0.7 %copy.9 = bf16[64,1024]{1,0:T(8,128)(2,1)} copy(bf16[64,1024]{1,0:T(8,128)(2,1)S(1)} %shard_map.73) | data formatting | bytes 262144
